TPU v7x, 32 devices: a whole 2x2x4 slice. The times are simulated.
32 devices in a mesh: sp: 8 (over z, x), tp: 4 (over y, core).
Axes of the slice: x: 2, y: 2, z: 4, core: 2. Of those that a mesh axis runs over, the one named last changes fastest.
Arguments:
- residual: bfloat16 [8192, 2048], P('sp'), may hold values from -6 to 6
- query: bfloat16 [8192, 1024], P('sp', 'tp'), may hold values from -6 to 6
- key: bfloat16 [8192, 256], P('sp', 'tp'), may hold values from -6 to 6
- value: bfloat16 [8192, 256], P('sp', 'tp'), may hold values from -6 to 6
- sink: float32 [16], P('tp'), may hold values from 3 to 9
- norm_gain: float32 [2048], replicated, may hold values from 0.1 to 1.9
- w_out: bfloat16 [1024, 2048], P('tp'), may hold values from -1.5 to 1.5
- w_gate: bfloat16 [2048, 4096], P('sp', 'tp'), may hold values from -0.125 to 0.125
- w_value: bfloat16 [2048, 4096], P('sp', 'tp'), may hold values from -0.125 to 0.125
- conv_gate: bfloat16 [3, 4096], P(None, 'tp'), may hold values from -3 to 3
- conv_value: bfloat16 [3, 4096], P(None, 'tp'), may hold values from -3 to 3
- w_down: bfloat16 [4096, 2048], P('tp', 'sp'), may hold values from -0.09375 to 0.09375
Outputs:
- layer_out: bfloat16 [8192, 2048], P(('sp', 'tp'))
All inputs are finite; a program needn't handle non-finite values.
Results may differ from a plain program's by a relative error of at most 0.015.
Values may be sent and summed in bfloat16 or wider, within the bound.
A program may use at most 128 MiB of HBM per device.

v0:
```python
import jax
import jax.numpy as jnp
from jax import lax
from jax.sharding import PartitionSpec as P

HD = 64
WINDOW = 128


THETA = 10000.0
EPS = 1e-06


def extended(block, sides, width):
    for axis, dim in sides:
        count = lax.axis_size(axis)
        forward = [(i, i + 1) for i in range(count - 1)]
        backward = [(target, source) for source, target in forward]
        low = lax.ppermute(
            lax.slice_in_dim(block, block.shape[dim] - width, None, axis=dim), axis, forward
        )
        high = lax.ppermute(lax.slice_in_dim(block, 0, width, axis=dim), axis, backward)
        block = jnp.concatenate([low, block, high], axis=dim)
    return block


def rotate(field, positions):
    count = field.shape[0]
    parts = field.astype(jnp.float32).reshape(count, -1, HD)
    inverse = 1.0 / THETA ** (jnp.arange(0, HD, 2, dtype=jnp.float32) / HD)
    angle = positions[:, None] * inverse[None, :]
    cosine = jnp.cos(angle)[:, None, :]
    sine = jnp.sin(angle)[:, None, :]
    first = parts[..., : HD // 2]
    second = parts[..., HD // 2 :]
    turned = jnp.concatenate(
        [first * cosine - second * sine, second * cosine + first * sine], axis=-1
    )
    return turned.reshape(count, -1).astype(jnp.bfloat16)


def band_attention(queries, keys, values, sinks, start, total):
    count = queries.shape[0]
    blocks = count // WINDOW
    kv_local = keys.shape[1] // HD
    group = queries.shape[1] // (kv_local * HD)
    query_blocks = queries.reshape(blocks, WINDOW, kv_local, group, HD)
    key_band = jnp.concatenate(
        [
            keys[i * WINDOW : i * WINDOW + count].reshape(blocks, WINDOW, kv_local, HD)
            for i in range(3)
        ],
        axis=1,
    )
    value_band = jnp.concatenate(
        [
            values[i * WINDOW : i * WINDOW + count].reshape(blocks, WINDOW, kv_local, HD)
            for i in range(3)
        ],
        axis=1,
    )
    scores = jnp.einsum(
        "nqkgd,njkd->nkgqj", query_blocks, key_band, preferred_element_type=jnp.float32
    ) * HD ** (-0.5)
    block_ids = jnp.arange(blocks, dtype=jnp.int32)[:, None]
    query_pos = start + block_ids * WINDOW + jnp.arange(WINDOW, dtype=jnp.int32)[None, :]
    key_pos = start - WINDOW + block_ids * WINDOW + jnp.arange(3 * WINDOW, dtype=jnp.int32)[None, :]
    valid = (
        (key_pos[:, None, :] >= 0)
        & (key_pos[:, None, :] < total)
        & (jnp.abs(query_pos[:, :, None] - key_pos[:, None, :]) <= WINDOW)
    )
    scores = jnp.where(valid[:, None, None], scores, -1e30)
    sink_col = sinks.reshape(1, kv_local, group, 1, 1)
    top = jnp.maximum(jnp.max(scores, axis=-1, keepdims=True), sink_col)
    weights = jnp.exp(scores - top)
    denom = jnp.sum(weights, axis=-1, keepdims=True) + jnp.exp(sink_col - top)
    probs = (weights / denom).astype(jnp.bfloat16)
    out = jnp.einsum("nkgqj,njkd->nqkgd", probs, value_band, preferred_element_type=jnp.float32)
    return out.reshape(count, kv_local * group * HD).astype(jnp.bfloat16)


def rmsnorm(field, gain):
    wide = field.astype(jnp.float32)
    scale = lax.rsqrt(jnp.mean(wide * wide, axis=-1, keepdims=True) + EPS)
    return (wide * scale * gain).astype(jnp.bfloat16)


def shards(
    residual,
    query,
    key,
    value,
    sink,
    norm_gain,
    w_out,
    w_gate,
    w_value,
    conv_gate,
    conv_value,
    w_down,
):
    tok_rows = query.shape[0]
    offset = lax.axis_index("sp") * tok_rows
    total = tok_rows * lax.axis_size("sp")
    share = tok_rows // lax.axis_size("tp")
    tp_index = lax.axis_index("tp")
    positions = (offset + jnp.arange(tok_rows, dtype=jnp.int32)).astype(jnp.float32)
    turned_query = rotate(query, positions)
    turned_key = rotate(key, positions)
    key_width = key.shape[1]
    band = jnp.concatenate([turned_key, value], axis=1)
    edged = extended(band, (("sp", 0),), WINDOW)
    attended = band_attention(
        turned_query, edged[:, :key_width], edged[:, key_width:], sink, offset, total
    )
    partial_value = jnp.dot(attended, w_out, preferred_element_type=jnp.float32)
    mix_full = lax.psum(partial_value.astype(jnp.bfloat16), "tp").astype(jnp.float32)
    mid_full = (residual.astype(jnp.float32) + mix_full).astype(jnp.bfloat16)
    normed = rmsnorm(mid_full, norm_gain)
    mid_rows = lax.dynamic_slice_in_dim(mid_full, tp_index * share, share, 0)
    gate_full, value_full = (
        lax.all_gather(w_gate, "sp", axis=0, tiled=True),
        lax.all_gather(w_value, "sp", axis=0, tiled=True),
    )
    gate_up = jnp.dot(normed, gate_full, preferred_element_type=jnp.float32).astype(jnp.bfloat16)
    value_up = jnp.dot(normed, value_full, preferred_element_type=jnp.float32).astype(jnp.bfloat16)
    hidden_width = gate_up.shape[1]
    stacked = jnp.concatenate([gate_up, value_up], axis=1)
    edged_up = extended(stacked, (("sp", 0),), 1).astype(jnp.float32)
    taps = jnp.concatenate([conv_gate, conv_value], axis=1).astype(jnp.float32)
    convolved = edged_up[:-2] * taps[0] + edged_up[1:-1] * taps[1] + edged_up[2:] * taps[2]
    hidden = (jax.nn.silu(convolved[:, :hidden_width]) * convolved[:, hidden_width:]).astype(
        jnp.bfloat16
    )
    terms = jnp.dot(
        hidden, lax.all_gather(w_down, "sp", axis=1, tiled=True), preferred_element_type=jnp.float32
    )
    ffn_rows = lax.psum_scatter(
        terms.astype(jnp.bfloat16), "tp", scatter_dimension=0, tiled=True
    ).astype(jnp.float32)
    return (mid_rows.astype(jnp.float32) + ffn_rows).astype(jnp.bfloat16)


def solution(mesh):
    return jax.shard_map(
        shards,
        mesh=mesh,
        in_specs=(
            P("sp", None),
            P("sp", "tp"),
            P("sp", "tp"),
            P("sp", "tp"),
            P("tp"),
            P(),
            P("tp", None),
            P("sp", "tp"),
            P("sp", "tp"),
            P(None, "tp"),
            P(None, "tp"),
            P("tp", "sp"),
        ),
        out_specs=P(("sp", "tp"), None),
        check_vma=False,
    )
```

profile of v0, /device:TPU:0, one launch (start us, length us, event | category | flops | bytes accessed | tf_op | source)
XLA Modules:
  0.0 336.9 jit_solution(1129287583386971566)
XLA Ops:
  9.8 4.9 %collective-permute-start = (bf16[128,128]{0,1:T(8,128)(2,1)S(1)}, bf16[128,128]{0,1:T(8,128)(2,1)S(1)}, u32[]{:S(2)}, u32[]{:S(2)}) collective-permute-start(bf16[128,128]{0,1:T(8,128)(2,1)S(1)} %get-tuple-element.19), channel_id=1, source_target_pairs={{0,4},{4,8},{8,12},{12,16},{16,20},{20,24},{24,28},{1,5},{5,9},{9,... | collective-permute-start | bytes 98312 | tf_op jit(solution)/shard_map/ppermute | solution.py:19
  14.7 1.3 collective-permute-start.1
  16.7 1.2 copy.20
  18.3 1.2 fusion.12
  20.7 1.0 fusion.6
  21.8 1.5 fusion.5
  23.5 1.9 fusion.16
  25.8 3.3 convolution_convert_fusion
  31.2 85.1 %all-reduce.2.cloned.1.call-done = bf16[1024,2048]{1,0:T(8,128)(2,1)} async-done(((bf16[1024,2048]{1,0:T(8,128)(2,1)}), bf16[1024,2048]{1,0:T(8,128)(2,1)}) %all-reduce.2.cloned.1.call-update) | async-done | bytes 4194320 | tf_op jit(solution)/shard_map/psum | solution.py:118
  116.2 7.4 %fusion = (f32[1024]{0:T(1024)S(1)}, bf16[1024,2048]{1,0:T(8,128)(2,1)}) fusion(bf16[1024,2048]{1,0:T(8,128)(2,1)} %all-reduce.2.cloned.1.call-done, bf16[1024,2048]{1,0:T(8,128)(2,1)} %param.12), kind=kLoop, calls=%fused_computation.2 | loop fusion | flops 14679040 | bytes 12587008 | tf_op jit(solution)/shard_map/reduce_sum | solution.py:85
  123.6 8.4 %convolution_convert_fusion.2 = bf16[1024,1024]{0,1:T(8,128)(2,1)S(1)} fusion(bf16[2048,1024]{1,0:T(8,128)(2,1)} %all-gather.6.cloned.1.call-done, bf16[1024,2048]{1,0:T(8,128)(2,1)} %get-tuple-element.6, f32[2048]{0:T(1024)S(1)} %copy-done.6, f32[1024]{0:T(1024)S(1)} %add_rsqrt_fusion), kind=kOutput, calls=%fused_computation.29 | convolution fusion | flops 4304404480 | bytes 10498048 | tf_op jit(solution)/shard_map/dot_general | solution.py:127
  132.1 46.9 %all-gather.4.cloned.1.call-done = bf16[2048,1024]{1,0:T(8,128)(2,1)} async-done(((bf16[256,1024]{1,0:T(8,128)(2,1)}), bf16[2048,1024]{1,0:T(8,128)(2,1)}) %all-gather.4.cloned.1.call-update) | async-done | bytes 4194320 | tf_op jit(solution)/shard_map/all_gather | solution.py:123
  179.0 8.4 %convolution_convert_fusion.3 = bf16[1024,1024]{0,1:T(8,128)(2,1)S(1)} fusion(bf16[2048,1024]{1,0:T(8,128)(2,1)} %all-gather.4.cloned.1.call-done, bf16[1024,2048]{1,0:T(8,128)(2,1)} %get-tuple-element.6, f32[2048]{0:T(1024)S(1)} %copy-done.6, f32[1024]{0:T(1024)S(1)} %add_rsqrt_fusion), kind=kOutput, calls=%fused_computation.30 | convolution fusion | flops 4304404480 | bytes 10498048 | tf_op jit(solution)/shard_map/dot_general | solution.py:126
  187.9 2.5 collective-permute-start.2
  190.4 1.3 collective-permute-start.3
  191.7 2.5 pad_maximum_fusion
  194.2 22.0 %collective-permute-done.2 = bf16[1,2048]{0,1:T(8,128)(2,1)S(1)} collective-permute-done((bf16[1,2048]{0,1:T(8,128)(2,1)S(1)}, bf16[1,2048]{0,1:T(8,128)(2,1)S(1)}, u32[]{:S(2)}, u32[]{:S(2)}) %collective-permute-start.2) | collective-permute-done | bytes 4128 | tf_op jit(solution)/shard_map/ppermute | solution.py:19
  216.1 9.3 %concatenate.42 = bf16[1026,2048]{0,1:T(8,128)(2,1)} concatenate(bf16[1,2048]{0,1:T(8,128)(2,1)S(1)} %collective-permute-done.2, bf16[1024,2048]{0,1:T(8,128)(2,1)} %pad_maximum_fusion, bf16[1,2048]{0,1:T(8,128)(2,1)} %collective-permute-done.3), dimensions={0} | concatenate | bytes 8404992 | tf_op jit(solution)/shard_map/concatenate | solution.py:23
  225.5 2.9 convert_element_type.108
  228.4 8.5 %fusion.3 = f32[1024,2048]{0,1:T(8,128)} fusion(f32[1026,2048]{0,1:T(8,128)S(1)} %convert_element_type.108, f32[2048]{0:T(1024)S(1)} %bitcast.117, f32[2048]{0:T(1024)S(1)} %bitcast.116, f32[2048]{0:T(1024)S(1)} %bitcast.115), kind=kLoop, calls=%fused_computation.6 | loop fusion | flops 10485760 | bytes 33579008 | tf_op jit(solution)/shard_map/add | solution.py:132
  236.9 35.2 %all-gather.8.cloned.1.call-done = bf16[1024,2048]{1,0:T(8,128)(2,1)} async-done(((bf16[1024,256]{1,0:T(8,128)(2,1)}), bf16[1024,2048]{1,0:T(8,128)(2,1)}) %all-gather.8.cloned.1.call-update) | async-done | bytes 4194320 | tf_op jit(solution)/shard_map/all_gather | solution.py:137
  272.1 11.4 %convolution_convert_fusion.1 = bf16[1024,2048]{1,0:T(8,128)(2,1)} fusion(bf16[1024,2048]{1,0:T(8,128)(2,1)} %all-gather.8.cloned.1.call-done, f32[1024,2048]{0,1:T(8,128)} %fusion.3), kind=kOutput, calls=%fused_computation.24 | convolution fusion | flops 4303355904 | bytes 16777216 | tf_op jit(solution)/shard_map/dot_general | solution.py:136
  283.5 42.9 %reduce-scatter.2.cloned.1.call-done = bf16[256,2048]{1,0:T(8,128)(2,1)} async-done(((bf16[1024,2048]{1,0:T(8,128)(2,1)}), bf16[256,2048]{1,0:T(8,128)(2,1)}) %reduce-scatter.2.cloned.1.call-update) | async-done | bytes 1048592 | tf_op jit(solution)/shard_map/reduce_scatter | solution.py:139
  326.4 2.9 add_convert_fusion.1
  (60 shorter events, 7.7 us)
Async XLA Ops:
  7.4 18.4 %copy-start = (bf16[256,2048]{1,0:T(8,128)(2,1)S(1)}, bf16[256,2048]{1,0:T(8,128)(2,1)}, u32[]{:S(2)}) copy-start(bf16[256,2048]{1,0:T(8,128)(2,1)} %param.18) | copy-start | bytes 3145732
  7.4 12.1 %copy-start.2 = (bf16[1024,64]{0,1:T(8,128)(2,1)S(1)}, bf16[1024,64]{0,1:T(8,128)(2,1)}, u32[]{:S(2)}) copy-start(bf16[1024,64]{0,1:T(8,128)(2,1)} %param.15) | copy-start | bytes 393220
  7.4 108.8 %all-reduce.2.cloned.1.call-start = ((), (), s32[]{:S(2)}) async-start(), calls=%async_computation.1 | async-start | bytes 8388608 | tf_op jit(solution)/shard_map/psum | solution.py:118
  9.8 9.7 %collective-permute-start = (bf16[128,128]{0,1:T(8,128)(2,1)S(1)}, bf16[128,128]{0,1:T(8,128)(2,1)S(1)}, u32[]{:S(2)}, u32[]{:S(2)}) collective-permute-start(bf16[128,128]{0,1:T(8,128)(2,1)S(1)} %get-tuple-element.19), channel_id=1, source_target_pairs={{0,4},{4,8},{8,12},{12,16},{16,20},{20,24},{24,28},{1,5},{5,9},{9,... | collective-permute-start | bytes 98312 | tf_op jit(solution)/shard_map/ppermute | solution.py:19
  14.7 5.8 %collective-permute-start.1 = (bf16[128,128]{0,1:T(8,128)(2,1)S(1)}, bf16[128,128]{0,1:T(8,128)(2,1)S(1)}, u32[]{:S(2)}, u32[]{:S(2)}) collective-permute-start(bf16[128,128]{0,1:T(8,128)(2,1)S(1)} %get-tuple-element.20), channel_id=1, source_target_pairs={{4,0},{8,4},{12,8},{16,12},{20,16},{24,20},{28,24},{5,1},{9,5},{13... | collective-permute-start | bytes 98312 | tf_op jit(solution)/shard_map/ppermute | solution.py:22
  20.7 1.1 copy-start.5
  29.1 2.0 copy-start.3
  29.1 2.0 copy-start.4
  29.1 94.5 %all-gather.6.cloned.1.call-start = ((), (), s32[]{:S(2)}) async-start(), calls=%async_computation.3 | async-start | bytes 4718592 | tf_op jit(solution)/shard_map/all_gather | solution.py:124
  29.7 149.3 %all-gather.4.cloned.1.call-start = ((), (), s32[]{:S(2)}) async-start(), calls=%async_computation.2 | async-start | bytes 4718592 | tf_op jit(solution)/shard_map/all_gather | solution.py:123
  30.3 241.9 %all-gather.8.cloned.1.call-start = ((), (), s32[]{:S(2)}) async-start(), calls=%async_computation.4 | async-start | bytes 4718592 | tf_op jit(solution)/shard_map/all_gather | solution.py:137
  30.9 295.6 %reduce-scatter.2.cloned.1.call-start = ((), (), s32[]{:S(2)}) async-start(), calls=%async_computation.5 | async-start | bytes 5242880 | tf_op jit(solution)/shard_map/reduce_scatter | solution.py:139
  31.1 92.5 %copy-start.6 = (f32[2048]{0:T(1024)S(1)}, f32[2048]{0:T(1024)}, u32[]{:S(2)}) copy-start(f32[2048]{0:T(1024)} %param.17) | copy-start | bytes 24580
  187.9 28.2 %collective-permute-start.2 = (bf16[1,2048]{0,1:T(8,128)(2,1)S(1)}, bf16[1,2048]{0,1:T(8,128)(2,1)S(1)}, u32[]{:S(2)}, u32[]{:S(2)}) collective-permute-start(bf16[1,2048]{0,1:T(8,128)(2,1)S(1)} %get-tuple-element.8), channel_id=1, source_target_pairs={{0,4},{4,8},{8,12},{12,16},{16,20},{20,24},{24,28},{1,5},{5,9},{9,... | collective-permute-start | bytes 12296 | tf_op jit(solution)/shard_map/ppermute | solution.py:19
  190.4 25.7 %collective-permute-start.3 = (bf16[1,2048]{0,1:T(8,128)(2,1)S(1)}, bf16[1,2048]{0,1:T(8,128)(2,1)}, u32[]{:S(2)}, u32[]{:S(2)}) collective-permute-start(bf16[1,2048]{0,1:T(8,128)(2,1)S(1)} %get-tuple-element.7), channel_id=1, source_target_pairs={{4,0},{8,4},{12,8},{16,12},{20,16},{24,20},{28,24},{5,1},{9,5},{13... | collective-permute-start | bytes 12296 | tf_op jit(solution)/shard_map/ppermute | solution.py:22
  272.1 57.2 %copy-start.1 = (bf16[256,2048]{1,0:T(8,128)(2,1)S(1)}, bf16[256,2048]{1,0:T(8,128)(2,1)}, u32[]{:S(2)}) copy-start(bf16[256,2048]{1,0:T(8,128)(2,1)} %param.18) | copy-start | bytes 3145732
Sparse Core Ops, SparseCore 0:
  29.2 86.9 all-reduce.1
  283.7 42.7 reduce-scatter.1
Sparse Core Ops, SparseCore 1:
  31.7 74.0 all-gather.5
  107.8 71.1 all-gather.3
  180.9 91.2 all-gather.7
where the time goes:
time: 338 us; the launch traced here: 337 us
  waiting for transfers between devices  235 us (70%)
  matrix products  34.4 us (10%)
  other arithmetic  31.1 us (9%)
  between operations  15.4 us (5%)
  local copies, waits for them, and re-layouts  11.2 us (3%)
  starting transfers between devices  10.3 us (3%)
    psum x1, waiting for transfers between devices, shards(): lax.psum(partial_value.astype(jnp.bfloat16), 'tp').astype(jnp.float32)  85.1 us
    all_gather x1, waiting for transfers between devices, shards(): lax.all_gather(w_gate, 'sp', axis=0, tiled=True)  46.9 us
    reduce_scatter x1, waiting for transfers between devices, shards(): lax.psum_scatter(terms.astype(jnp.bfloat16), 'tp', scatter_dimension=0, t...  42.9 us
    all_gather x1, waiting for transfers between devices, shards(): lax.all_gather(w_down, 'sp', axis=1, tiled=True)  35.2 us
    ppermute x2, waiting for transfers between devices, extended(): lax.ppermute(lax.slice_in_dim(block, block.shape[dim] - width, None, axis...  22 us
    dot_general x1, matrix products, shards(): jnp.dot(hidden, lax.all_gather(w_down, 'sp', axis=1, tiled=True), preferr...  11.4 us
    concatenate x1, local copies, waits for them, and re-layouts, extended(): block = jnp.concatenate([low, block, high], axis=dim)  9.35 us
    add x1, other arithmetic, shards(): edged_up[:-2] * taps[0] + edged_up[1:-1] * taps[1] + edged_up[2:] * taps[2]  8.49 us
  transfers between devices with their start and end apart: 9, of which 6 were waited for; matrix products, arithmetic and copies ran while one was open for 15% of the time, Pallas kernels for 0%

commit v1 on v0

--- a/solution.py
+++ b/solution.py
@@ -1,6 +1,10 @@
+import functools
+
 import jax
 import jax.numpy as jnp
 from jax import lax
+from jax.experimental import pallas as pl
+from jax.experimental.pallas import tpu as pltpu
 from jax.sharding import PartitionSpec as P
 
 HD = 64
@@ -86,7 +90,7 @@
     return (wide * scale * gain).astype(jnp.bfloat16)
 
 
-def shards(
+def plain_shards(
     residual,
     query,
     key,
@@ -142,7 +146,561 @@
     return (mid_rows.astype(jnp.float32) + ffn_rows).astype(jnp.bfloat16)
 
 
+F32 = jnp.float32
+BF16 = jnp.bfloat16
+PAIR = 2
+EDGE = 8
+
+
+def layer_kernel(
+    sp,
+    tp,
+    q_ref,
+    band_ref,
+    sink_ref,
+    res_ref,
+    gain_ref,
+    wo_ref,
+    wg_ref,
+    wv_ref,
+    tg_ref,
+    tv_ref,
+    wd_ref,
+    out_ref,
+    band,
+    att,
+    wo,
+    wg,
+    wv,
+    wd,
+    mid,
+    normed,
+    upg,
+    upv,
+    hidden,
+    terms,
+    rbuf,
+    local_sem,
+    up_send,
+    up_recv,
+    dn_send,
+    dn_recv,
+    wo_send,
+    wo_recv,
+    att_send,
+    att_recv,
+    kv_send,
+    kv_recv,
+    edge_send,
+    edge_recv,
+    rs_send,
+    rs_recv,
+):
+    me = lax.axis_index("sp")
+    my_tp = lax.axis_index("tp")
+    tok = res_ref.shape[0]
+    width = res_ref.shape[1]
+    share = tok // tp
+    line = sp // PAIR
+    place = me // PAIR
+    side = me % PAIR
+    mate = place * PAIR + (1 - side)
+    depth = wg_ref.shape[0]
+    cols = wd_ref.shape[1]
+    hid = wg_ref.shape[1]
+    has_low = me > 0
+    has_high = me < sp - 1
+    can_down = place > 0
+    can_up = place < line - 1
+    peers = [lax.rem(my_tp + k, tp) for k in range(1, tp)]
+
+    def remote(src, dst, send, recv, **where):
+        return pltpu.make_async_remote_copy(
+            src_ref=src,
+            dst_ref=dst,
+            send_sem=send,
+            recv_sem=recv,
+            device_id=where,
+            device_id_type=pl.DeviceIdType.MESH,
+        )
+
+    barrier = pltpu.get_barrier_semaphore()
+
+    def greet(**where):
+        pl.semaphore_signal(
+            barrier, inc=1, device_id=where, device_id_type=pl.DeviceIdType.MESH
+        )
+
+    greet(sp=mate)
+    for peer in peers:
+        greet(tp=peer)
+    far_low = has_low & (side == 0)
+    far_high = has_high & (side == PAIR - 1)
+    pl.when(far_low)(lambda: greet(sp=me - 1))
+    pl.when(far_high)(lambda: greet(sp=me + 1))
+    pl.when(can_down)(lambda: greet(sp=me - PAIR))
+    pl.when(can_up)(lambda: greet(sp=me + PAIR))
+    count = tp
+    for able in (far_low, far_high, can_down, can_up):
+        count = count + jnp.where(able, 1, 0)
+    pl.semaphore_wait(barrier, count)
+
+    def up_slot(kind, block):
+        return (wg, wv)[kind].at[pl.ds(pl.multiple_of(block * depth, depth), depth), :]
+
+    def up_copy(kind, block, way, own=False):
+        target = (me - PAIR, me + PAIR, mate)[way]
+        slot = up_slot(kind, block)
+        return remote(
+            (wg_ref, wv_ref)[kind] if own else slot,
+            slot,
+            up_send.at[kind, block, way],
+            up_recv.at[kind, block],
+            sp=target,
+        )
+
+    def dn_copy(block, way, own=False):
+        target = (me - PAIR, me + PAIR, mate)[way]
+        slot = wd.at[block]
+        return remote(
+            wd_ref if own else slot, slot, dn_send.at[block, way], dn_recv.at[block], sp=target
+        )
+
+    def candidate(c):
+        distance = (c + 1) // 2
+        there = jnp.where(c % 2 == 1, place + distance, place - distance)
+        valid = (there >= 0) & (there < line)
+        above = there > place
+        return there, valid, above
+
+    own_local = [
+        pltpu.make_async_copy(wg_ref, up_slot(0, me), local_sem.at[0]),
+        pltpu.make_async_copy(wv_ref, up_slot(1, me), local_sem.at[1]),
+        pltpu.make_async_copy(wd_ref, wd.at[me], local_sem.at[2]),
+        pltpu.make_async_copy(wo_ref, wo.at[my_tp], local_sem.at[3]),
+        pltpu.make_async_copy(band_ref, band.at[pl.ds(WINDOW, tok), :], local_sem.at[4]),
+    ]
+
+    kv_low = remote(
+        band_ref.at[pl.ds(0, WINDOW), :],
+        band.at[pl.ds(WINDOW + tok, WINDOW), :],
+        kv_send.at[0],
+        kv_recv.at[1],
+        sp=me - 1,
+    )
+    kv_high = remote(
+        band_ref.at[pl.ds(tok - WINDOW, WINDOW), :],
+        band.at[pl.ds(0, WINDOW), :],
+        kv_send.at[1],
+        kv_recv.at[0],
+        sp=me + 1,
+    )
+    pl.when(has_low)(kv_low.start)
+    pl.when(has_high)(kv_high.start)
+    for copy in own_local:
+        copy.start()
+    for kind in range(2):
+        up_copy(kind, me, 2, True).start()
+        pl.when(can_down)(up_copy(kind, me, 0, True).start)
+        pl.when(can_up)(up_copy(kind, me, 1, True).start)
+
+    def wo_copy(k):
+        return remote(wo_ref, wo.at[my_tp], wo_send.at[k], wo_recv.at[my_tp], tp=peers[k])
+
+    for k in range(tp - 1):
+        wo_copy(k).start()
+
+    blank = jnp.zeros((WINDOW, band.shape[1]), BF16)
+
+    @pl.when(jnp.logical_not(has_low))
+    def _():
+        band[pl.ds(0, WINDOW), :] = blank
+
+    @pl.when(jnp.logical_not(has_high))
+    def _():
+        band[pl.ds(WINDOW + tok, WINDOW), :] = blank
+
+    own_local[4].wait()
+    pl.when(has_low)(kv_high.wait_recv)
+    pl.when(has_high)(kv_low.wait_recv)
+    heads = q_ref.shape[0]
+    span = 3 * WINDOW
+    total = tok * sp
+
+    def attend(i, carry):
+        start = pl.multiple_of(i * WINDOW, WINDOW)
+        keys = band[pl.ds(start, span), :]
+        row = lax.broadcasted_iota(jnp.int32, (WINDOW, span), 0)
+        col = lax.broadcasted_iota(jnp.int32, (WINDOW, span), 1)
+        key_pos = col + (me * tok - WINDOW + start)
+        valid = (col >= row) & (col <= row + 2 * WINDOW) & (key_pos >= 0) & (key_pos < total)
+        lane = lax.broadcasted_iota(jnp.int32, (WINDOW, 2 * HD), 1)
+        outs = []
+        for h in range(heads):
+            scores = lax.dot_general(
+                q_ref[h, pl.ds(start, WINDOW), :],
+                keys,
+                (((1,), (1,)), ((), ())),
+                preferred_element_type=F32,
+            )
+            scores = jnp.where(valid, scores, -1e30)
+            sink = sink_ref[h]
+            top = jnp.maximum(jnp.max(scores, axis=-1, keepdims=True), sink)
+            weights = jnp.exp(scores - top)
+            denom = jnp.sum(weights, axis=-1, keepdims=True) + jnp.exp(sink - top)
+            probs = (weights * (1.0 / denom)).astype(BF16)
+            outs.append(jnp.dot(probs, keys, preferred_element_type=F32))
+        for h in range(0, heads, 2):
+            pair = jnp.where(lane < HD, pltpu.roll(outs[h], HD, 1), outs[h + 1])
+            att[my_tp, pl.ds(start, WINDOW), pl.ds(h * HD, 2 * HD)] = pair.astype(BF16)
+        return carry
+
+    lax.fori_loop(0, tok // WINDOW, attend, 0)
+
+    def att_copy(k):
+        return remote(
+            att.at[my_tp], att.at[my_tp], att_send.at[k], att_recv.at[my_tp], tp=peers[k]
+        )
+
+    for k in range(tp - 1):
+        att_copy(k).start()
+
+    def pass_up(c, carry):
+        there, valid, above = candidate(c)
+        block = there * PAIR + side
+
+        @pl.when(valid)
+        def _():
+            for kind in range(2):
+                up_copy(kind, block, 2).wait_recv()
+                up_copy(kind, block, 2).start()
+                pl.when(above & can_down)(up_copy(kind, block, 0).start)
+                pl.when(jnp.logical_not(above) & can_up)(up_copy(kind, block, 1).start)
+
+        return carry
+
+    def start_down():
+        dn_copy(me, 2, True).start()
+        pl.when(can_down)(dn_copy(me, 0, True).start)
+        pl.when(can_up)(dn_copy(me, 1, True).start)
+
+    lax.fori_loop(1, 2 * line - 1, pass_up, 0)
+    start_down()
+
+    own_local[3].wait()
+    for k in range(tp - 1):
+        src = peers[k]
+        remote(wo_ref, wo.at[src], wo_send.at[k], wo_recv.at[src], tp=src).wait_recv()
+        remote(att.at[src], att.at[src], att_send.at[k], att_recv.at[src], tp=src).wait_recv()
+    tile = tok // 4
+    piece = 512
+
+    def mix(i, carry):
+        rows = pl.ds(pl.multiple_of(i * tile, tile), tile)
+        squares = jnp.zeros((tile, 1), F32)
+        for c in range(0, width, piece):
+            acc = jnp.zeros((tile, piece), F32)
+            for k in range(tp):
+                term = jnp.dot(
+                    att[k, rows, :], wo[k, :, pl.ds(c, piece)], preferred_element_type=F32
+                )
+                acc = acc + term.astype(BF16).astype(F32)
+            new = (res_ref[rows, pl.ds(c, piece)].astype(F32) + acc).astype(BF16)
+            mid[rows, pl.ds(c, piece)] = new
+            wide = new.astype(F32)
+            squares = squares + jnp.sum(wide * wide, axis=-1, keepdims=True)
+        scale = lax.rsqrt(squares * (1.0 / width) + EPS)
+        for c in range(0, width, piece):
+            wide = mid[rows, pl.ds(c, piece)].astype(F32)
+            normed[rows, pl.ds(c, piece)] = (
+                wide * scale * gain_ref[:, pl.ds(c, piece)]
+            ).astype(BF16)
+        return carry
+
+    lax.fori_loop(0, 4, mix, 0)
+
+    for kind in range(2):
+        own_local[kind].wait()
+
+    def take_up(c, carry):
+        there, valid, above = candidate(c)
+
+        @pl.when(valid)
+        def _():
+            for kind in range(2):
+                up_copy(kind, there * PAIR + (1 - side), 2).wait_recv()
+
+        return carry
+
+    lax.fori_loop(0, 2 * line - 1, take_up, 0)
+
+    def project(i, carry):
+        base = pl.multiple_of(i * tile, tile)
+        left = normed[pl.ds(base, tile), :]
+        rows = pl.ds(pl.multiple_of(base + EDGE, EDGE), tile)
+        for weight, dest in ((wg, upg), (wv, upv)):
+            for c in range(0, hid, piece):
+                term = jnp.dot(left, weight[:, pl.ds(c, piece)], preferred_element_type=F32)
+                dest[rows, pl.ds(c, piece)] = term.astype(BF16).astype(F32)
+        return carry
+
+    lax.fori_loop(0, 4, project, 0)
+
+    def edge_low(kind):
+        ref = (upg, upv)[kind]
+        return remote(
+            ref.at[pl.ds(EDGE, EDGE), :],
+            ref.at[pl.ds(EDGE + tok, EDGE), :],
+            edge_send.at[0, kind],
+            edge_recv.at[1, kind],
+            sp=me - 1,
+        )
+
+    def edge_high(kind):
+        ref = (upg, upv)[kind]
+        return remote(
+            ref.at[pl.ds(tok, EDGE), :],
+            ref.at[pl.ds(0, EDGE), :],
+            edge_send.at[1, kind],
+            edge_recv.at[0, kind],
+            sp=me + 1,
+        )
+
+    none = jnp.zeros((EDGE, hid), F32)
+    for kind in range(2):
+        pl.when(has_low)(edge_low(kind).start)
+        pl.when(has_high)(edge_high(kind).start)
+
+    @pl.when(jnp.logical_not(has_low))
+    def _():
+        upg[pl.ds(0, EDGE), :] = none
+        upv[pl.ds(0, EDGE), :] = none
+
+    @pl.when(jnp.logical_not(has_high))
+    def _():
+        upg[pl.ds(EDGE + tok, EDGE), :] = none
+        upv[pl.ds(EDGE + tok, EDGE), :] = none
+
+    for kind in range(2):
+        pl.when(has_low)(edge_high(kind).wait_recv)
+        pl.when(has_high)(edge_low(kind).wait_recv)
+
+    def gate(i, carry):
+        base = pl.multiple_of(i * WINDOW, WINDOW)
+        for c in range(0, hid, 256):
+            lanes = pl.ds(c, 256)
+
+            def convolve(ref, taps):
+                field = ref[pl.ds(base, WINDOW + 2 * EDGE), lanes]
+                return (
+                    field[EDGE - 1 : EDGE - 1 + WINDOW] * taps[0:1, lanes]
+                    + field[EDGE : EDGE + WINDOW] * taps[1:2, lanes]
+                    + field[EDGE + 1 : EDGE + 1 + WINDOW] * taps[2:3, lanes]
+                )
+
+            g = convolve(upg, tg_ref)
+            v = convolve(upv, tv_ref)
+            hidden[pl.ds(base, WINDOW), lanes] = (g / (1.0 + jnp.exp(-g)) * v).astype(BF16)
+        return carry
+
+    lax.fori_loop(0, tok // WINDOW, gate, 0)
+
+    def rs_copy(block, k):
+        return remote(
+            terms.at[block, pl.ds(pl.multiple_of(peers[k] * share, share), share), :],
+            rbuf.at[my_tp, block],
+            rs_send.at[block, k],
+            rs_recv.at[block, my_tp],
+            tp=peers[k],
+        )
+
+    def process(block):
+        def part(i, carry):
+            rows = pl.ds(pl.multiple_of(i * tile, tile), tile)
+            terms[block, rows, :] = jnp.dot(
+                hidden[rows, :], wd[block], preferred_element_type=F32
+            ).astype(BF16)
+            return carry
+
+        lax.fori_loop(0, 4, part, 0)
+        for k in range(tp - 1):
+            rs_copy(block, k).start()
+
+    own_local[2].wait()
+
+    def down(c, carry):
+        there, valid, above = candidate(c)
+        block = there * PAIR + side
+
+        @pl.when(valid)
+        def _():
+            @pl.when(c > 0)
+            def _():
+                dn_copy(block, 2).wait_recv()
+                dn_copy(block, 2).start()
+                pl.when(above & can_down)(dn_copy(block, 0).start)
+                pl.when(jnp.logical_not(above) & can_up)(dn_copy(block, 1).start)
+
+            process(block)
+
+        before, was_valid, _ = candidate(jnp.maximum(c - 1, 0))
+
+        @pl.when(was_valid & (c > 0))
+        def _():
+            other = before * PAIR + (1 - side)
+            dn_copy(other, 2).wait_recv()
+            process(other)
+
+        return carry
+
+    lax.fori_loop(0, 2 * line, down, 0)
+
+    my_rows = pl.ds(pl.multiple_of(my_tp * share, share), share)
+
+    for block in range(sp):
+        lanes = pl.ds(block * cols, cols)
+        acc = mid[my_rows, lanes].astype(F32) + terms[block, my_rows, :].astype(F32)
+        for k in range(tp - 1):
+            src = peers[k]
+            remote(
+                rbuf.at[src, block],
+                rbuf.at[src, block],
+                rs_send.at[block, k],
+                rs_recv.at[block, src],
+                tp=src,
+            ).wait_recv()
+            acc = acc + rbuf[src, block].astype(F32)
+        out_ref[:, lanes] = acc.astype(BF16)
+
+    def drain(c, carry):
+        there, valid, above = candidate(c)
+        block = there * PAIR + side
+        goes_down = can_down & (above | (c == 0))
+        goes_up = can_up & (jnp.logical_not(above) | (c == 0))
+
+        @pl.when(valid)
+        def _():
+            for copy in (
+                lambda way: up_copy(0, block, way),
+                lambda way: up_copy(1, block, way),
+                lambda way: dn_copy(block, way),
+            ):
+                copy(2).wait_send()
+                pl.when(goes_down)(copy(0).wait_send)
+                pl.when(goes_up)(copy(1).wait_send)
+
+        return carry
+
+    lax.fori_loop(0, 2 * line - 1, drain, 0)
+    for k in range(tp - 1):
+        wo_copy(k).wait_send()
+        att_copy(k).wait_send()
+    pl.when(has_low)(kv_low.wait_send)
+    pl.when(has_high)(kv_high.wait_send)
+    for kind in range(2):
+        pl.when(has_low)(edge_low(kind).wait_send)
+        pl.when(has_high)(edge_high(kind).wait_send)
+
+    def drain_rs(block, carry):
+        for k in range(tp - 1):
+            rs_copy(block, k).wait_send()
+        return carry
+
+    lax.fori_loop(0, sp, drain_rs, 0)
+
+
+def kernel_shards(
+    sp,
+    tp,
+    residual,
+    query,
+    key,
+    value,
+    sink,
+    norm_gain,
+    w_out,
+    w_gate,
+    w_value,
+    conv_gate,
+    conv_value,
+    w_down,
+):
+    tok, width = residual.shape
+    depth, hid = w_gate.shape
+    cols = w_down.shape[1]
+    heads = query.shape[1] // HD
+    offset = lax.axis_index("sp") * tok
+    positions = (offset + jnp.arange(tok, dtype=jnp.int32)).astype(F32)
+    turned_query = rotate(query, positions) * jnp.asarray(HD**-0.5, BF16)
+    turned_key = rotate(key, positions)
+    band = jnp.concatenate([turned_key, value], axis=1)
+    by_head = turned_query.reshape(tok, heads, HD).transpose(1, 0, 2)
+    by_head = jnp.pad(by_head, ((0, 0), (0, 0), (0, HD)))
+    vmem = pl.BlockSpec(memory_space=pltpu.VMEM)
+    smem = pl.BlockSpec(memory_space=pltpu.SMEM)
+    dma = pltpu.SemaphoreType.DMA
+    return pl.pallas_call(
+        functools.partial(layer_kernel, sp, tp),
+        out_shape=jax.ShapeDtypeStruct((tok // tp, width), BF16),
+        in_specs=[vmem, vmem, smem] + [vmem] * 8,
+        out_specs=vmem,
+        scratch_shapes=[
+            pltpu.VMEM((tok + 2 * WINDOW, 2 * HD), BF16),
+            pltpu.VMEM((tp, tok, heads * HD), BF16),
+            pltpu.VMEM((tp,) + w_out.shape, BF16),
+            pltpu.VMEM((sp * depth, hid), BF16),
+            pltpu.VMEM((sp * depth, hid), BF16),
+            pltpu.VMEM((sp, hid, cols), BF16),
+            pltpu.VMEM((tok, width), BF16),
+            pltpu.VMEM((tok, width), BF16),
+            pltpu.VMEM((tok + 2 * EDGE, hid), F32),
+            pltpu.VMEM((tok + 2 * EDGE, hid), F32),
+            pltpu.VMEM((tok, hid), BF16),
+            pltpu.VMEM((sp, tok, cols), BF16),
+            pltpu.VMEM((tp, sp, tok // tp, cols), BF16),
+            dma((5,)),
+            dma((2, sp, 3)),
+            dma((2, sp)),
+            dma((sp, 3)),
+            dma((sp,)),
+            dma((tp - 1,)),
+            dma((tp,)),
+            dma((tp - 1,)),
+            dma((tp,)),
+            dma((2,)),
+            dma((2,)),
+            dma((2, 2)),
+            dma((2, 2)),
+            dma((sp, tp - 1)),
+            dma((sp, tp)),
+        ],
+        compiler_params=pltpu.CompilerParams(
+            collective_id=0, has_side_effects=True, vmem_limit_bytes=66 * 1000 * 1000
+        ),
+        name="layer",
+    )(
+        by_head,
+        band,
+        sink,
+        residual,
+        norm_gain.reshape(1, -1),
+        w_out,
+        w_gate,
+        w_value,
+        conv_gate.astype(F32),
+        conv_value.astype(F32),
+        w_down,
+    )
+
+
 def solution(mesh):
+    sp, tp = mesh.shape["sp"], mesh.shape["tp"]
+
+    def shards(*args):
+        if args[11].shape[1] % 128 or sp % PAIR:
+            return plain_shards(*args)
+        return kernel_shards(sp, tp, *args)
+
     return jax.shard_map(
         shards,
         mesh=mesh,

time: 338 us -> 197 us (0.58)
  the two profiles are of different devices: /device:TPU:0 before, /device:TPU:29 now
where the time goes in v1:
time: 197 us
  Pallas kernels  177 us (90%)
  local copies, waits for them, and re-layouts  10.8 us (5%)
  other arithmetic  9.35 us (5%)
    pallas_call x1, Pallas kernels, kernel_shards(): pl.pallas_call(functools.partial(layer_kernel, sp, tp), out_shape=jax.Sha...  177 us
    unnamed x14, local copies, waits for them, and re-layouts  8.55 us
    another operation x2, other arithmetic  4.55 us

profile of v1, /device:TPU:29, one launch (start us, length us, event | category | flops | bytes accessed | tf_op | source)
XLA Modules:
  0.0 196.9 jit_solution(13046883193083651519)
XLA Ops:
  0.0 1.9 multiply_cosine_fusion.1
  1.9 1.2 copy.20
  3.2 1.1 fusion.9
  4.2 1.6 copy.26
  5.9 3.0 %copy.27 = f32[1024,4,32]{2,0,1:T(8,128)} copy(f32[1024,4,32]{0,2,1:T(8,128)} %get-tuple-element.9) | data formatting | bytes 1048576
  8.9 2.1 %subtract_convert_fusion = (bf16[1024,4,32]{2,0,1:T(8,128)(2,1)S(1)}, bf16[1024,4,32]{2,0,1:T(8,128)(2,1)S(1)}) fusion(f32[1024,4,32]{2,0,1:T(8,128)} %copy.27, f32[1024,4,32]{2,0,1:T(8,128)S(1)} %copy.26, f32[1024,32]{1,0:T(8,128)S(1)} %get-tuple-element.12, f32[1024,32]{1,0:T(8,128)S(1)} %get-tuple-element.11), kind=kLoop, calls=%fused_computation.1 | loop fusion | flops 1048576 | bytes 1835008 | tf_op jit(solution)/shard_map/convert.4
  11.0 0.0 copy-start
  11.0 0.6 fusion
  11.7 1.2 pad.4.q_ref
  12.9 0.0 copy-done
  12.9 0.2 copy.23
  13.1 0.0 copy-start.2
  13.1 0.0 copy-start.3
  13.1 2.4 %fusion.6 = (bf16[1024,1,32]{2,0,1:T(8,128)(2,1)S(1)}, bf16[1024,1,32]{2,0,1:T(8,128)(2,1)S(1)}) fusion(f32[1024,1,64]{2,0,1:T(8,128)S(1)} %bitcast_convert_fusion, f32[1024]{0:T(1024)S(1)} %add_convert_fusion.1, f32[32]{0:T(128)S(1)} %negate_power_fusion), kind=kLoop, calls=%fused_computation.13 | loop fusion | flops 294912 | bytes 397440 | tf_op jit(solution)/shard_map/convert.2
  15.6 0.1 maximum_bitcast_fusion
  15.7 0.0 copy-done.1
  15.7 0.2 copy.25
  15.9 0.9 pad_maximum_fusion.band_ref
  16.7 0.0 copy-done.2
  16.8 0.6 convert_element_type.25.tg_ref
  17.4 0.0 copy-done.3
  17.4 0.6 convert_element_type.26.tv_ref
  18.0 176.6 %layer.1 = bf16[256,2048]{1,0:T(8,128)(2,1)} custom-call(bf16[4,1024,128]{2,1,0:T(8,128)(2,1)} %pad.4.q_ref, bf16[1024,128]{1,0:T(8,128)(2,1)} %pad_maximum_fusion.band_ref, f32[4]{0:T(128)} %sink_ref.1, bf16[1024,2048]{1,0:T(8,128)(2,1)} %res_ref.1, f32[1,2048]{1,0:T(1,128)} %bitcast.11, bf16[256,2048]{1,0:T(8,128)(2,1)} %wo_ref.1, ...), custom_call_target="tpu_custom_call" | custom-call | tf_op jit(solution)/shard_map/layer/pallas_call | solution.py:642
  194.6 2.3 %copy.29 = bf16[256,2048]{1,0:T(8,128)(2,1)} copy(bf16[256,2048]{1,0:T(8,128)(2,1)} %layer.1) | data formatting | bytes 2097152
  (4 shorter events, 0.1 us)
Async XLA Ops:
  11.0 1.8 copy-start
  12.9 2.8 %copy-start.1 = (bf16[1024,64]{0,1:T(8,128)(2,1)S(1)}, bf16[1024,64]{0,1:T(8,128)(2,1)}, u32[]{:S(2)}) copy-start(bf16[1024,64]{0,1:T(8,128)(2,1)} %param.15) | copy-start | bytes 393220
  13.1 3.7 %copy-start.2 = (bf16[3,1024]{1,0:T(4,128)(2,1)S(1)}, bf16[3,1024]{1,0:T(4,128)(2,1)}, u32[]{:S(2)}) copy-start(bf16[3,1024]{1,0:T(4,128)(2,1)} %param.21) | copy-start | bytes 18436
  13.1 4.3 %copy-start.3 = (bf16[3,1024]{1,0:T(4,128)(2,1)S(1)}, bf16[3,1024]{1,0:T(4,128)(2,1)}, u32[]{:S(2)}) copy-start(bf16[3,1024]{1,0:T(4,128)(2,1)} %param.22) | copy-start | bytes 18436

commit v2 on v1

--- a/solution.py
+++ b/solution.py
@@ -2,6 +2,7 @@
 
 import jax
 import jax.numpy as jnp
+import numpy as np
 from jax import lax
 from jax.experimental import pallas as pl
 from jax.experimental.pallas import tpu as pltpu
@@ -157,6 +158,9 @@
     tp,
     q_ref,
     band_ref,
+    cos_ref,
+    sin_ref,
+    base_ref,
     sink_ref,
     res_ref,
     gain_ref,
@@ -168,6 +172,8 @@
     wd_ref,
     out_ref,
     band,
+    key_value,
+    value_key,
     att,
     wo,
     wg,
@@ -179,7 +185,9 @@
     upv,
     hidden,
     terms,
-    rbuf,
+    near,
+    pair_sum,
+    far,
     local_sem,
     up_send,
     up_recv,
@@ -193,13 +201,14 @@
     kv_recv,
     edge_send,
     edge_recv,
-    rs_send,
-    rs_recv,
+    near_send,
+    near_recv,
+    far_send,
+    far_recv,
 ):
     me = lax.axis_index("sp")
     my_tp = lax.axis_index("tp")
-    tok = res_ref.shape[0]
-    width = res_ref.shape[1]
+    tok, width = mid.shape
     share = tok // tp
     line = sp // PAIR
     place = me // PAIR
@@ -212,7 +221,10 @@
     has_high = me < sp - 1
     can_down = place > 0
     can_up = place < line - 1
-    peers = [lax.rem(my_tp + k, tp) for k in range(1, tp)]
+    buddy = my_tp + 1 - 2 * (my_tp % 2)
+    across = lax.rem(my_tp + 2, tp)
+    corner = lax.rem(buddy + 2, tp)
+    peers = [buddy, across, corner]
 
     def remote(src, dst, send, recv, **where):
         return pltpu.make_async_remote_copy(
@@ -273,12 +285,16 @@
         above = there > place
         return there, valid, above
 
+    def distance_of(there):
+        return jnp.where(there > place, there - place, place - there)
+
     own_local = [
         pltpu.make_async_copy(wg_ref, up_slot(0, me), local_sem.at[0]),
         pltpu.make_async_copy(wv_ref, up_slot(1, me), local_sem.at[1]),
         pltpu.make_async_copy(wd_ref, wd.at[me], local_sem.at[2]),
         pltpu.make_async_copy(wo_ref, wo.at[my_tp], local_sem.at[3]),
         pltpu.make_async_copy(band_ref, band.at[pl.ds(WINDOW, tok), :], local_sem.at[4]),
+        pltpu.make_async_copy(res_ref, mid, local_sem.at[5]),
     ]
 
     kv_low = remote(
@@ -304,11 +320,32 @@
         pl.when(can_down)(up_copy(kind, me, 0, True).start)
         pl.when(can_up)(up_copy(kind, me, 1, True).start)
 
-    def wo_copy(k):
-        return remote(wo_ref, wo.at[my_tp], wo_send.at[k], wo_recv.at[my_tp], tp=peers[k])
-
-    for k in range(tp - 1):
-        wo_copy(k).start()
+    def wo_copy(k, own=True):
+        slot = wo.at[my_tp if own else across]
+        return remote(
+            wo_ref if own else slot,
+            slot,
+            wo_send.at[k],
+            wo_recv.at[my_tp if own else across],
+            tp=(buddy, across, buddy)[k],
+        )
+
+    def att_copy(k):
+        slot = att.at[across if k == 2 else my_tp]
+        return remote(
+            slot,
+            slot,
+            att_send.at[k],
+            att_recv.at[across if k == 2 else my_tp],
+            tp=(buddy, across, buddy)[k],
+        )
+
+    def arrived(ref, recv, source):
+        slot = ref.at[source]
+        return remote(slot, slot, wo_send.at[0], recv.at[source], tp=buddy)
+
+    wo_copy(1).start()
+    wo_copy(0).start()
 
     blank = jnp.zeros((WINDOW, band.shape[1]), BF16)
 
@@ -323,47 +360,69 @@
     own_local[4].wait()
     pl.when(has_low)(kv_high.wait_recv)
     pl.when(has_high)(kv_low.wait_recv)
-    heads = q_ref.shape[0]
+    heads = q_ref.shape[1] // HD
     span = 3 * WINDOW
     total = tok * sp
+    lane = lax.broadcasted_iota(jnp.int32, (WINDOW, 2 * HD), 1)
+    early = lane % HD < HD // 2
+    low = lane < HD
+
+    def turn(field, start):
+        rows = pl.ds(start, WINDOW)
+        base_cos = base_ref[0:1, :]
+        base_sin = base_ref[1:2, :]
+        cosine = base_cos * cos_ref[rows, :] - base_sin * sin_ref[rows, :]
+        sine = base_sin * cos_ref[rows, :] + base_cos * sin_ref[rows, :]
+        ahead = pltpu.roll(field, 2 * HD - HD // 2, 1)
+        behind = pltpu.roll(field, HD // 2, 1)
+        return field * cosine + jnp.where(early, -ahead, behind) * sine
+
+    def turn_keys(i, carry):
+        start = pl.multiple_of(i * WINDOW, WINDOW)
+        field = band[pl.ds(start, WINDOW), :].astype(F32)
+        field = jnp.where(low, turn(field, start), field)
+        key_value[pl.ds(start, WINDOW), :] = field.astype(BF16)
+        value_key[pl.ds(start, WINDOW), :] = pltpu.roll(field, HD, 1).astype(BF16)
+        return carry
+
+    lax.fori_loop(0, tok // WINDOW + 2, turn_keys, 0)
 
     def attend(i, carry):
         start = pl.multiple_of(i * WINDOW, WINDOW)
-        keys = band[pl.ds(start, span), :]
+        straight = key_value[pl.ds(start, span), :]
+        crossed = value_key[pl.ds(start, span), :]
         row = lax.broadcasted_iota(jnp.int32, (WINDOW, span), 0)
         col = lax.broadcasted_iota(jnp.int32, (WINDOW, span), 1)
         key_pos = col + (me * tok - WINDOW + start)
         valid = (col >= row) & (col <= row + 2 * WINDOW) & (key_pos >= 0) & (key_pos < total)
-        lane = lax.broadcasted_iota(jnp.int32, (WINDOW, 2 * HD), 1)
-        outs = []
-        for h in range(heads):
+
+        def head(query, sink, keys, values):
             scores = lax.dot_general(
-                q_ref[h, pl.ds(start, WINDOW), :],
-                keys,
-                (((1,), (1,)), ((), ())),
-                preferred_element_type=F32,
+                query, keys, (((1,), (1,)), ((), ())), preferred_element_type=F32
             )
             scores = jnp.where(valid, scores, -1e30)
-            sink = sink_ref[h]
             top = jnp.maximum(jnp.max(scores, axis=-1, keepdims=True), sink)
             weights = jnp.exp(scores - top)
             denom = jnp.sum(weights, axis=-1, keepdims=True) + jnp.exp(sink - top)
             probs = (weights * (1.0 / denom)).astype(BF16)
-            outs.append(jnp.dot(probs, keys, preferred_element_type=F32))
+            return jnp.dot(probs, values, preferred_element_type=F32)
+
         for h in range(0, heads, 2):
-            pair = jnp.where(lane < HD, pltpu.roll(outs[h], HD, 1), outs[h + 1])
-            att[my_tp, pl.ds(start, WINDOW), pl.ds(h * HD, 2 * HD)] = pair.astype(BF16)
+            lanes = pl.ds(h * HD, 2 * HD)
+            field = q_ref[pl.ds(start, WINDOW), lanes].astype(F32)
+            field = turn(field, pl.multiple_of(start + WINDOW, WINDOW)) * HD**-0.5
+            even = head(
+                jnp.where(low, field, 0.0).astype(BF16), sink_ref[h], straight, crossed
+            )
+            odd = head(
+                jnp.where(low, 0.0, field).astype(BF16), sink_ref[h + 1], crossed, straight
+            )
+            att[my_tp, pl.ds(start, WINDOW), lanes] = jnp.where(low, even, odd).astype(BF16)
         return carry
 
     lax.fori_loop(0, tok // WINDOW, attend, 0)
-
-    def att_copy(k):
-        return remote(
-            att.at[my_tp], att.at[my_tp], att_send.at[k], att_recv.at[my_tp], tp=peers[k]
-        )
-
-    for k in range(tp - 1):
-        att_copy(k).start()
+    att_copy(1).start()
+    att_copy(0).start()
 
     def pass_up(c, carry):
         there, valid, above = candidate(c)
@@ -373,7 +432,8 @@
         def _():
             for kind in range(2):
                 up_copy(kind, block, 2).wait_recv()
-                up_copy(kind, block, 2).start()
+                direct = (kind == 1) | (distance_of(there) > 1)
+                pl.when(direct)(up_copy(kind, block, 2).start)
                 pl.when(above & can_down)(up_copy(kind, block, 0).start)
                 pl.when(jnp.logical_not(above) & can_up)(up_copy(kind, block, 1).start)
 
@@ -384,14 +444,35 @@
         pl.when(can_down)(dn_copy(me, 0, True).start)
         pl.when(can_up)(dn_copy(me, 1, True).start)
 
-    lax.fori_loop(1, 2 * line - 1, pass_up, 0)
+    def pass_down(c, carry):
+        there, valid, above = candidate(c)
+        block = there * PAIR + side
+
+        @pl.when(valid)
+        def _():
+            dn_copy(block, 2).wait_recv()
+            dn_copy(block, 2).start()
+            pl.when(above & can_down)(dn_copy(block, 0).start)
+            pl.when(jnp.logical_not(above) & can_up)(dn_copy(block, 1).start)
+
+        return carry
+
+    up_copy(0, mate, 2).wait_recv()
+    pl.when(can_down)(up_copy(0, mate, 0).start)
+    pl.when(can_up)(up_copy(0, mate, 1).start)
+    lax.fori_loop(1, 3, pass_up, 0)
+    arrived(wo, wo_recv, across).wait_recv()
+    wo_copy(2, False).start()
+    arrived(att, att_recv, across).wait_recv()
+    att_copy(2).start()
+    lax.fori_loop(3, 2 * line - 1, pass_up, 0)
     start_down()
 
     own_local[3].wait()
-    for k in range(tp - 1):
-        src = peers[k]
-        remote(wo_ref, wo.at[src], wo_send.at[k], wo_recv.at[src], tp=src).wait_recv()
-        remote(att.at[src], att.at[src], att_send.at[k], att_recv.at[src], tp=src).wait_recv()
+    own_local[5].wait()
+    for source in (buddy, corner):
+        arrived(wo, wo_recv, source).wait_recv()
+        arrived(att, att_recv, source).wait_recv()
     tile = tok // 4
     piece = 512
 
@@ -405,7 +486,7 @@
                     att[k, rows, :], wo[k, :, pl.ds(c, piece)], preferred_element_type=F32
                 )
                 acc = acc + term.astype(BF16).astype(F32)
-            new = (res_ref[rows, pl.ds(c, piece)].astype(F32) + acc).astype(BF16)
+            new = (mid[rows, pl.ds(c, piece)].astype(F32) + acc).astype(BF16)
             mid[rows, pl.ds(c, piece)] = new
             wide = new.astype(F32)
             squares = squares + jnp.sum(wide * wide, axis=-1, keepdims=True)
@@ -427,8 +508,9 @@
 
         @pl.when(valid)
         def _():
-            for kind in range(2):
-                up_copy(kind, there * PAIR + (1 - side), 2).wait_recv()
+            other = there * PAIR + (1 - side)
+            pl.when(c > 0)(up_copy(0, other, 2).wait_recv)
+            up_copy(1, other, 2).wait_recv()
 
         return carry
 
@@ -467,6 +549,7 @@
         )
 
     none = jnp.zeros((EDGE, hid), F32)
+    lax.fori_loop(1, 3, pass_down, 0)
     for kind in range(2):
         pl.when(has_low)(edge_low(kind).start)
         pl.when(has_high)(edge_high(kind).start)
@@ -492,10 +575,11 @@
 
             def convolve(ref, taps):
                 field = ref[pl.ds(base, WINDOW + 2 * EDGE), lanes]
+                taps = taps[:, lanes].astype(F32)
                 return (
-                    field[EDGE - 1 : EDGE - 1 + WINDOW] * taps[0:1, lanes]
-                    + field[EDGE : EDGE + WINDOW] * taps[1:2, lanes]
-                    + field[EDGE + 1 : EDGE + 1 + WINDOW] * taps[2:3, lanes]
+                    field[EDGE - 1 : EDGE - 1 + WINDOW] * taps[0:1]
+                    + field[EDGE : EDGE + WINDOW] * taps[1:2]
+                    + field[EDGE + 1 : EDGE + 1 + WINDOW] * taps[2:3]
                 )
 
             g = convolve(upg, tg_ref)
@@ -505,14 +589,28 @@
 
     lax.fori_loop(0, tok // WINDOW, gate, 0)
 
-    def rs_copy(block, k):
+    def rows_of(owner):
+        return pl.ds(pl.multiple_of(owner * share, share), share)
+
+    def near_copy(block, k):
         return remote(
-            terms.at[block, pl.ds(pl.multiple_of(peers[k] * share, share), share), :],
-            rbuf.at[my_tp, block],
-            rs_send.at[block, k],
-            rs_recv.at[block, my_tp],
-            tp=peers[k],
-        )
+            terms.at[block, rows_of((buddy, corner)[k]), :],
+            near.at[k, block],
+            near_send.at[block, k],
+            near_recv.at[block, k],
+            tp=buddy,
+        )
+
+    def far_copy(block):
+        return remote(
+            pair_sum.at[block], far.at[block], far_send.at[block], far_recv.at[block], tp=across
+        )
+
+    def pass_pair(block):
+        near_copy(block, 1).wait_recv()
+        both = terms[block, rows_of(across), :].astype(F32) + near[1, block].astype(F32)
+        pair_sum[block] = both.astype(BF16)
+        far_copy(block).start()
 
     def process(block):
         def part(i, carry):
@@ -523,8 +621,8 @@
             return carry
 
         lax.fori_loop(0, 4, part, 0)
-        for k in range(tp - 1):
-            rs_copy(block, k).start()
+        near_copy(block, 1).start()
+        near_copy(block, 0).start()
 
     own_local[2].wait()
 
@@ -534,12 +632,9 @@
 
         @pl.when(valid)
         def _():
-            @pl.when(c > 0)
+            @pl.when(c > 2)
             def _():
-                dn_copy(block, 2).wait_recv()
-                dn_copy(block, 2).start()
-                pl.when(above & can_down)(dn_copy(block, 0).start)
-                pl.when(jnp.logical_not(above) & can_up)(dn_copy(block, 1).start)
+                pass_down(c, 0)
 
             process(block)
 
@@ -550,26 +645,26 @@
             other = before * PAIR + (1 - side)
             dn_copy(other, 2).wait_recv()
             process(other)
-
-        return carry
-
-    lax.fori_loop(0, 2 * line, down, 0)
+            pass_pair(before * PAIR + side)
+
+        earlier, was_valid, _ = candidate(jnp.maximum(c - 2, 0))
+
+        @pl.when(was_valid & (c > 1))
+        def _():
+            pass_pair(earlier * PAIR + (1 - side))
+
+        return carry
+
+    lax.fori_loop(0, 2 * line + 1, down, 0)
 
     my_rows = pl.ds(pl.multiple_of(my_tp * share, share), share)
 
     for block in range(sp):
         lanes = pl.ds(block * cols, cols)
         acc = mid[my_rows, lanes].astype(F32) + terms[block, my_rows, :].astype(F32)
-        for k in range(tp - 1):
-            src = peers[k]
-            remote(
-                rbuf.at[src, block],
-                rbuf.at[src, block],
-                rs_send.at[block, k],
-                rs_recv.at[block, src],
-                tp=src,
-            ).wait_recv()
-            acc = acc + rbuf[src, block].astype(F32)
+        near_copy(block, 0).wait_recv()
+        far_copy(block).wait_recv()
+        acc = acc + near[0, block].astype(F32) + far[block].astype(F32)
         out_ref[:, lanes] = acc.astype(BF16)
 
     def drain(c, carry):
@@ -580,20 +675,25 @@
 
         @pl.when(valid)
         def _():
-            for copy in (
-                lambda way: up_copy(0, block, way),
-                lambda way: up_copy(1, block, way),
-                lambda way: dn_copy(block, way),
+            direct = (distance_of(there) > 1) | (c == 0)
+            for kind, copy in enumerate(
+                (
+                    lambda way: up_copy(0, block, way),
+                    lambda way: up_copy(1, block, way),
+                    lambda way: dn_copy(block, way),
+                )
             ):
-                copy(2).wait_send()
+                pl.when(direct | (kind > 0))(copy(2).wait_send)
                 pl.when(goes_down)(copy(0).wait_send)
                 pl.when(goes_up)(copy(1).wait_send)
 
         return carry
 
+    pl.when(can_down)(up_copy(0, mate, 0).wait_send)
+    pl.when(can_up)(up_copy(0, mate, 1).wait_send)
     lax.fori_loop(0, 2 * line - 1, drain, 0)
     for k in range(tp - 1):
-        wo_copy(k).wait_send()
+        wo_copy(k, k < 2).wait_send()
         att_copy(k).wait_send()
     pl.when(has_low)(kv_low.wait_send)
     pl.when(has_high)(kv_high.wait_send)
@@ -602,8 +702,9 @@
         pl.when(has_high)(edge_high(kind).wait_send)
 
     def drain_rs(block, carry):
-        for k in range(tp - 1):
-            rs_copy(block, k).wait_send()
+        near_copy(block, 0).wait_send()
+        near_copy(block, 1).wait_send()
+        far_copy(block).wait_send()
         return carry
 
     lax.fori_loop(0, sp, drain_rs, 0)
@@ -629,22 +730,25 @@
     depth, hid = w_gate.shape
     cols = w_down.shape[1]
     heads = query.shape[1] // HD
+    share = tok // tp
     offset = lax.axis_index("sp") * tok
-    positions = (offset + jnp.arange(tok, dtype=jnp.int32)).astype(F32)
-    turned_query = rotate(query, positions) * jnp.asarray(HD**-0.5, BF16)
-    turned_key = rotate(key, positions)
-    band = jnp.concatenate([turned_key, value], axis=1)
-    by_head = turned_query.reshape(tok, heads, HD).transpose(1, 0, 2)
-    by_head = jnp.pad(by_head, ((0, 0), (0, 0), (0, HD)))
+    band = jnp.concatenate([key, value], axis=1)
+    inverse = THETA ** (-(np.arange(2 * HD) % (HD // 2)) * 2.0 / HD)
+    angle = (np.arange(tok + 2 * WINDOW) - WINDOW)[:, None] * inverse[None, :]
+    first = offset.astype(F32) * jnp.asarray(inverse, F32)
+    base = jnp.stack([jnp.cos(first), jnp.sin(first)])
     vmem = pl.BlockSpec(memory_space=pltpu.VMEM)
     smem = pl.BlockSpec(memory_space=pltpu.SMEM)
+    anywhere = pl.BlockSpec(memory_space=pl.ANY)
     dma = pltpu.SemaphoreType.DMA
     return pl.pallas_call(
         functools.partial(layer_kernel, sp, tp),
         out_shape=jax.ShapeDtypeStruct((tok // tp, width), BF16),
-        in_specs=[vmem, vmem, smem] + [vmem] * 8,
+        in_specs=[vmem] * 5 + [smem, anywhere, vmem] + [anywhere] * 3 + [vmem] * 2 + [anywhere],
         out_specs=vmem,
         scratch_shapes=[
+            pltpu.VMEM((tok + 2 * WINDOW, 2 * HD), BF16),
+            pltpu.VMEM((tok + 2 * WINDOW, 2 * HD), BF16),
             pltpu.VMEM((tok + 2 * WINDOW, 2 * HD), BF16),
             pltpu.VMEM((tp, tok, heads * HD), BF16),
             pltpu.VMEM((tp,) + w_out.shape, BF16),
@@ -657,8 +761,10 @@
             pltpu.VMEM((tok + 2 * EDGE, hid), F32),
             pltpu.VMEM((tok, hid), BF16),
             pltpu.VMEM((sp, tok, cols), BF16),
-            pltpu.VMEM((tp, sp, tok // tp, cols), BF16),
-            dma((5,)),
+            pltpu.VMEM((2, sp, share, cols), BF16),
+            pltpu.VMEM((sp, share, cols), BF16),
+            pltpu.VMEM((sp, share, cols), BF16),
+            dma((6,)),
             dma((2, sp, 3)),
             dma((2, sp)),
             dma((sp, 3)),
@@ -671,24 +777,29 @@
             dma((2,)),
             dma((2, 2)),
             dma((2, 2)),
-            dma((sp, tp - 1)),
-            dma((sp, tp)),
+            dma((sp, 2)),
+            dma((sp, 2)),
+            dma((sp,)),
+            dma((sp,)),
         ],
         compiler_params=pltpu.CompilerParams(
             collective_id=0, has_side_effects=True, vmem_limit_bytes=66 * 1000 * 1000
         ),
         name="layer",
     )(
-        by_head,
+        query,
         band,
+        jnp.asarray(np.cos(angle), F32),
+        jnp.asarray(np.sin(angle), F32),
+        base,
         sink,
         residual,
         norm_gain.reshape(1, -1),
         w_out,
         w_gate,
         w_value,
-        conv_gate.astype(F32),
-        conv_value.astype(F32),
+        conv_gate,
+        conv_value,
         w_down,
     )
 
@@ -697,7 +808,7 @@
     sp, tp = mesh.shape["sp"], mesh.shape["tp"]
 
     def shards(*args):
-        if args[11].shape[1] % 128 or sp % PAIR:
+        if args[11].shape[1] % 128 or sp % PAIR or tp != 4 or args[2].shape[1] != HD:
             return plain_shards(*args)
         return kernel_shards(sp, tp, *args)
 

time: 197 us -> 178 us (0.904)
  the two profiles are of different devices: /device:TPU:29 before, /device:TPU:0 now
where the time goes in v2:
time: 178 us; the launch traced here: 177 us
  Pallas kernels  170 us (96%)
  local copies, waits for them, and re-layouts  4.45 us (2%)
  other arithmetic  2.15 us (1%)
    pallas_call x1, Pallas kernels, kernel_shards(): pl.pallas_call(functools.partial(layer_kernel, sp, tp), out_shape=jax.Sha...  170 us
    unnamed x3, local copies, waits for them, and re-layouts  4.45 us

profile of v2, /device:TPU:0, one launch (start us, length us, event | category | flops | bytes accessed | tf_op | source)
XLA Modules:
  0.0 176.8 jit_solution(13407644880780730299)
XLA Ops:
  0.0 0.7 fusion
  0.7 0.6 pad_maximum_fusion.1.base_ref
  1.3 1.1 copy.16
  2.4 1.1 copy.17
  3.5 0.9 pad_maximum_fusion.band_ref
  4.3 170.2 %layer.1 = bf16[256,2048]{1,0:T(8,128)(2,1)} custom-call(bf16[1024,256]{1,0:T(8,128)(2,1)} %q_ref.1, bf16[1024,128]{1,0:T(8,128)(2,1)} %pad_maximum_fusion.band_ref, f32[1280,128]{1,0:T(8,128)} %constant.15.clone.cos_ref, f32[1280,128]{1,0:T(8,128)} %constant.16.clone.sin_ref, f32[2,128]{1,0:T(2,128)} %pad_maximum_fusion.1.base_ref, f32[4]{0:T(128)} %sink_ref.1, ...), custom_call_target="tpu_custom_call" | custom-call | tf_op jit(solution)/shard_map/layer/pallas_call | solution.py:744
  174.5 2.3 %copy.19 = bf16[256,2048]{1,0:T(8,128)(2,1)} copy(bf16[256,2048]{1,0:T(8,128)(2,1)} %layer.1) | data formatting | bytes 2097152

commit v3 on v2

--- a/solution.py
+++ b/solution.py
@@ -150,6 +150,8 @@
 F32 = jnp.float32
 BF16 = jnp.bfloat16
 PAIR = 2
+HALVES = 2
+PIECES = 2 * HALVES
 EDGE = 8
 
 
@@ -215,6 +217,7 @@
     side = me % PAIR
     mate = place * PAIR + (1 - side)
     depth = wg_ref.shape[0]
+    half = depth // HALVES
     cols = wd_ref.shape[1]
     hid = wg_ref.shape[1]
     has_low = me > 0
@@ -258,13 +261,16 @@
     pl.semaphore_wait(barrier, count)
 
     def up_slot(kind, block):
-        return (wg, wv)[kind].at[pl.ds(pl.multiple_of(block * depth, depth), depth), :]
+        start = pl.multiple_of(block * depth + kind % HALVES * half, half)
+        return (wg, wv)[kind // HALVES].at[pl.ds(start, half), :]
 
     def up_copy(kind, block, way, own=False):
         target = (me - PAIR, me + PAIR, mate)[way]
         slot = up_slot(kind, block)
         return remote(
-            (wg_ref, wv_ref)[kind] if own else slot,
+            (wg_ref, wv_ref)[kind // HALVES].at[pl.ds(kind % HALVES * half, half), :]
+            if own
+            else slot,
             slot,
             up_send.at[kind, block, way],
             up_recv.at[kind, block],
@@ -288,9 +294,12 @@
     def distance_of(there):
         return jnp.where(there > place, there - place, place - there)
 
+    def up_rows(ref):
+        return ref.at[pl.ds(pl.multiple_of(me * depth, depth), depth), :]
+
     own_local = [
-        pltpu.make_async_copy(wg_ref, up_slot(0, me), local_sem.at[0]),
-        pltpu.make_async_copy(wv_ref, up_slot(1, me), local_sem.at[1]),
+        pltpu.make_async_copy(wg_ref, up_rows(wg), local_sem.at[0]),
+        pltpu.make_async_copy(wv_ref, up_rows(wv), local_sem.at[1]),
         pltpu.make_async_copy(wd_ref, wd.at[me], local_sem.at[2]),
         pltpu.make_async_copy(wo_ref, wo.at[my_tp], local_sem.at[3]),
         pltpu.make_async_copy(band_ref, band.at[pl.ds(WINDOW, tok), :], local_sem.at[4]),
@@ -315,10 +324,11 @@
     pl.when(has_high)(kv_high.start)
     for copy in own_local:
         copy.start()
-    for kind in range(2):
+    for kind in range(PIECES):
         up_copy(kind, me, 2, True).start()
         pl.when(can_down)(up_copy(kind, me, 0, True).start)
         pl.when(can_up)(up_copy(kind, me, 1, True).start)
+    dn_copy(me, 2, True).start()
 
     def wo_copy(k, own=True):
         slot = wo.at[my_tp if own else across]
@@ -424,23 +434,19 @@
     att_copy(1).start()
     att_copy(0).start()
 
-    def pass_up(c, carry):
+    def pass_up(c, kind):
         there, valid, above = candidate(c)
         block = there * PAIR + side
 
         @pl.when(valid)
         def _():
-            for kind in range(2):
-                up_copy(kind, block, 2).wait_recv()
-                direct = (kind == 1) | (distance_of(there) > 1)
-                pl.when(direct)(up_copy(kind, block, 2).start)
-                pl.when(above & can_down)(up_copy(kind, block, 0).start)
-                pl.when(jnp.logical_not(above) & can_up)(up_copy(kind, block, 1).start)
-
-        return carry
+            up_copy(kind, block, 2).wait_recv()
+            if c > 2 or kind >= HALVES:
+                up_copy(kind, block, 2).start()
+            pl.when(above & can_down)(up_copy(kind, block, 0).start)
+            pl.when(jnp.logical_not(above) & can_up)(up_copy(kind, block, 1).start)
 
     def start_down():
-        dn_copy(me, 2, True).start()
         pl.when(can_down)(dn_copy(me, 0, True).start)
         pl.when(can_up)(dn_copy(me, 1, True).start)
 
@@ -457,15 +463,21 @@
 
         return carry
 
-    up_copy(0, mate, 2).wait_recv()
-    pl.when(can_down)(up_copy(0, mate, 0).start)
-    pl.when(can_up)(up_copy(0, mate, 1).start)
-    lax.fori_loop(1, 3, pass_up, 0)
+    for kind in range(PIECES):
+        for c in (1, 2):
+            pass_up(c, kind)
+    for kind in range(HALVES):
+        up_copy(kind, mate, 2).wait_recv()
+        pl.when(can_down)(up_copy(kind, mate, 0).start)
+        pl.when(can_up)(up_copy(kind, mate, 1).start)
     arrived(wo, wo_recv, across).wait_recv()
     wo_copy(2, False).start()
     arrived(att, att_recv, across).wait_recv()
     att_copy(2).start()
-    lax.fori_loop(3, 2 * line - 1, pass_up, 0)
+    for kind in range(PIECES):
+        for c in (3, 4):
+            if c < 2 * line - 1:
+                pass_up(c, kind)
     start_down()
 
     own_local[3].wait()
@@ -500,6 +512,11 @@
 
     lax.fori_loop(0, 4, mix, 0)
 
+    for c in range(5, 2 * line - 1):
+        for kind in range(PIECES):
+            pass_up(c, kind)
+    lax.fori_loop(1, 3, pass_down, 0)
+
     for kind in range(2):
         own_local[kind].wait()
 
@@ -509,8 +526,11 @@
         @pl.when(valid)
         def _():
             other = there * PAIR + (1 - side)
-            pl.when(c > 0)(up_copy(0, other, 2).wait_recv)
-            up_copy(1, other, 2).wait_recv()
+            for kind in range(PIECES):
+                if kind < HALVES:
+                    pl.when(c > 0)(up_copy(kind, other, 2).wait_recv)
+                else:
+                    up_copy(kind, other, 2).wait_recv()
 
         return carry
 
@@ -549,7 +569,7 @@
         )
 
     none = jnp.zeros((EDGE, hid), F32)
-    lax.fori_loop(1, 3, pass_down, 0)
+    lax.fori_loop(3, min(5, 2 * line - 1), pass_down, 0)
     for kind in range(2):
         pl.when(has_low)(edge_low(kind).start)
         pl.when(has_high)(edge_high(kind).start)
@@ -632,7 +652,7 @@
 
         @pl.when(valid)
         def _():
-            @pl.when(c > 2)
+            @pl.when(c > 4)
             def _():
                 pass_down(c, 0)
 
@@ -676,21 +696,20 @@
         @pl.when(valid)
         def _():
             direct = (distance_of(there) > 1) | (c == 0)
-            for kind, copy in enumerate(
-                (
-                    lambda way: up_copy(0, block, way),
-                    lambda way: up_copy(1, block, way),
-                    lambda way: dn_copy(block, way),
-                )
-            ):
-                pl.when(direct | (kind > 0))(copy(2).wait_send)
+            for kind in range(PIECES + 1):
+                if kind < PIECES:
+                    copy = functools.partial(up_copy, kind, block)
+                else:
+                    copy = functools.partial(dn_copy, block)
+                pl.when(direct | (kind >= HALVES))(copy(2).wait_send)
                 pl.when(goes_down)(copy(0).wait_send)
                 pl.when(goes_up)(copy(1).wait_send)
 
         return carry
 
-    pl.when(can_down)(up_copy(0, mate, 0).wait_send)
-    pl.when(can_up)(up_copy(0, mate, 1).wait_send)
+    for kind in range(HALVES):
+        pl.when(can_down)(up_copy(kind, mate, 0).wait_send)
+        pl.when(can_up)(up_copy(kind, mate, 1).wait_send)
     lax.fori_loop(0, 2 * line - 1, drain, 0)
     for k in range(tp - 1):
         wo_copy(k, k < 2).wait_send()
@@ -765,8 +784,8 @@
             pltpu.VMEM((sp, share, cols), BF16),
             pltpu.VMEM((sp, share, cols), BF16),
             dma((6,)),
-            dma((2, sp, 3)),
-            dma((2, sp)),
+            dma((PIECES, sp, 3)),
+            dma((PIECES, sp)),
             dma((sp, 3)),
             dma((sp,)),
             dma((tp - 1,)),

time: 178 us -> 168 us (0.944)
  Pallas kernels: 170 us -> 161 us
    pallas_call x1, Pallas kernels: 170 us -> 161 us  [kernel_shards(): pl.pallas_call(functools.partial(layer_kernel, sp, tp), out_shape=jax.Sha...]
where the time goes in v3:
time: 168 us
  Pallas kernels  161 us (96%)
  local copies, waits for them, and re-layouts  4.45 us (3%)
  other arithmetic  2.15 us (1%)
    pallas_call x1, Pallas kernels, kernel_shards(): pl.pallas_call(functools.partial(layer_kernel, sp, tp), out_shape=jax.Sha...  161 us
    unnamed x3, local copies, waits for them, and re-layouts  4.45 us

profile of v3, /device:TPU:0, one launch (start us, length us, event | category | flops | bytes accessed | tf_op | source)
XLA Modules:
  0.0 167.8 jit_solution(12617112692398196545)
XLA Ops:
  0.0 0.7 fusion
  0.7 0.6 pad_maximum_fusion.1.base_ref
  1.3 1.1 copy.16
  2.4 1.1 copy.17
  3.5 0.9 pad_maximum_fusion.band_ref
  4.3 161.1 %layer.1 = bf16[256,2048]{1,0:T(8,128)(2,1)} custom-call(bf16[1024,256]{1,0:T(8,128)(2,1)} %q_ref.1, bf16[1024,128]{1,0:T(8,128)(2,1)} %pad_maximum_fusion.band_ref, f32[1280,128]{1,0:T(8,128)} %constant.15.clone.cos_ref, f32[1280,128]{1,0:T(8,128)} %constant.16.clone.sin_ref, f32[2,128]{1,0:T(2,128)} %pad_maximum_fusion.1.base_ref, f32[4]{0:T(128)} %sink_ref.1, ...), custom_call_target="tpu_custom_call" | custom-call | tf_op jit(solution)/shard_map/layer/pallas_call | solution.py:763
  165.5 2.3 %copy.19 = bf16[256,2048]{1,0:T(8,128)(2,1)} copy(bf16[256,2048]{1,0:T(8,128)(2,1)} %layer.1) | data formatting | bytes 2097152
